TPU v7x, 512 devices: a whole 4x4x16 slice. The times are simulated.
512 devices in a mesh: ep: 16 (over y, x), tp: 32 (over z, core).
Axes of the slice: x: 4, y: 4, z: 16, core: 2. Of those that a mesh axis runs over, the one named last changes fastest.
Arguments:
- tokens: bfloat16 [2048, 4096], P('ep', 'tp'), may hold values from -16 to 16
- routing: int32 [2048, 4], P('ep'), may hold values from 0 to 31, all different within a row; in each aligned block of 128 rows (0 to 127, 128 to 255, ...) at most 32 rows name the same one
- gate_weights: float32 [2048, 4], P('ep'), may hold values from 0.1 to 1
- w_gate: bfloat16 [32, 1024, 4096], P('ep', 'tp'), may hold values from -0.09375 to 0.09375
- w_up: bfloat16 [32, 1024, 4096], P('ep', 'tp'), may hold values from -0.09375 to 0.09375
- w_down: bfloat16 [32, 1024, 4096], P('ep', None, 'tp'), may hold values from -2 to 2
- out_gain: float32 [4096], P('tp'), may hold values from 0.1 to 1.9
Outputs:
- mixed: bfloat16 [2048, 4096], P('ep', 'tp')
Inputs may be any that keep to these rules, and one draw needn't show every extreme that they name: `routing`: in each aligned block of 128 rows (the tokens of one index of ep) no expert is named by more than 32 entries, and in every draw some expert is named by exactly 32 entries of some block. The 4 entries of a row differ.
All inputs are finite; a program needn't handle non-finite values.
Results may differ from a plain program's by a relative error of at most 0.0057.
Values may be sent and summed in bfloat16 or wider, within the bound.
A program may use at most 64 MiB of HBM per device.

v0:
```python
import jax
import jax.numpy as jnp
from jax import lax
from jax.sharding import PartitionSpec as P

D = 4096
TOPK = 4
EXP_DEV = 2
norm_eps = 1e-05


def from_everyone(value, axis):
    length = lax.axis_size(axis)
    return lax.all_to_all(
        jnp.broadcast_to(value[None], (length, *value.shape)), axis, 0, 0, tiled=True
    )


def taken_together(value, axis):
    return from_everyone(value, axis).sum(axis=0)


def body(tokens, routing, gate_weights, w_gate, w_up, w_down, out_gain):
    ep_count = lax.axis_size("ep")
    tok_rows = tokens.shape[0]
    width_part = tokens.shape[1]
    experts = EXP_DEV * ep_count
    slot_count = 2 * tok_rows * TOPK // experts
    span_rows = ep_count * slot_count
    total_slots = EXP_DEV * span_rows
    flat_route = routing.reshape(-1)
    expert_ids = jnp.arange(experts, dtype=jnp.int32)
    hit_table = (flat_route[:, None] == expert_ids[None, :]).astype(jnp.int32)
    running = jnp.cumsum(hit_table, axis=0) - hit_table
    slot_rank = jnp.sum(running * hit_table, axis=1)
    slot_target = flat_route % EXP_DEV * span_rows + flat_route // EXP_DEV * slot_count + slot_rank
    entry_targets = slot_target.reshape(tok_rows, TOPK)
    slot_ids = jnp.arange(total_slots, dtype=jnp.int32)
    select_table = jnp.any(entry_targets[None, :, :] == slot_ids[:, None, None], axis=2).astype(
        jnp.bfloat16
    )
    outgoing = jnp.dot(select_table, tokens, preferred_element_type=jnp.float32).astype(
        jnp.bfloat16
    )
    outgoing = outgoing.reshape(EXP_DEV, ep_count, slot_count, width_part)
    arrived = lax.all_to_all(outgoing, "ep", split_axis=1, concat_axis=1, tiled=True).reshape(
        EXP_DEV, span_rows, width_part
    )
    piece_cols = lax.all_gather(arrived, "tp", axis=2, tiled=True)
    gate_sum = jnp.einsum("efn,esn->efs", w_gate, piece_cols, preferred_element_type=jnp.float32)
    up_sum = jnp.einsum("efn,esn->efs", w_up, piece_cols, preferred_element_type=jnp.float32)
    square_sum = jnp.einsum(
        "esn,esn->es", piece_cols, piece_cols, preferred_element_type=jnp.float32
    )
    row_scale = lax.rsqrt(square_sum / D + norm_eps)[:, None, :]
    hidden = (jax.nn.silu(gate_sum * row_scale) * (up_sum * row_scale)).astype(jnp.bfloat16)
    out_part = w_down.shape[2]
    expert_out = jnp.einsum(
        "ens,end->esd",
        lax.all_gather(hidden, "tp", axis=1, tiled=True),
        w_down,
        preferred_element_type=jnp.float32,
    ).astype(jnp.bfloat16)
    returned = lax.all_to_all(
        expert_out.reshape(EXP_DEV, ep_count, slot_count, out_part),
        "ep",
        split_axis=1,
        concat_axis=1,
        tiled=True,
    )
    returned = returned.reshape(total_slots, out_part)
    chosen = returned[slot_target].astype(jnp.float32).reshape(tok_rows, TOPK, out_part)
    combined = jnp.sum(chosen * gate_weights[:, :, None], axis=1)
    square_total = taken_together(jnp.sum(combined * combined, axis=1), "tp")
    final_scale = lax.rsqrt(square_total / D + norm_eps)
    return (combined * final_scale[:, None] * out_gain[None, :]).astype(jnp.bfloat16)


def solution(mesh):
    placed = (
        P("ep", "tp"),
        P("ep", None),
        P("ep", None),
        P("ep", "tp", None),
        P("ep", "tp", None),
        P("ep", None, "tp"),
        P("tp"),
    )
    return jax.shard_map(body, mesh=mesh, in_specs=placed, out_specs=P("ep", "tp"), check_vma=False)
```

profile of v0, /device:TPU:1, one launch (start us, length us, event | category | flops | bytes accessed | tf_op | source)
XLA Modules:
  0.0 253.4 jit_solution(5410838036807146994)
XLA Ops:
  6.5 0.9 copy.73
  7.4 0.1 eq.44
  7.5 0.1 eq.40
  7.6 1.2 reduce-window.6
  8.8 0.2 slice_reduce_fusion
  9.1 0.1 fusion.9
  9.2 0.1 reduce_sum.41
  9.3 0.1 copy.76
  9.4 0.7 fusion.13
  10.1 0.4 fusion.1
  10.4 1.0 convolution_convert_fusion.1
  11.5 14.9 %all_to_all.16 = bf16[2,16,32,128]{3,2,0,1:T(8,128)(2,1)S(1)} all-to-all(bf16[2,16,32,128]{3,2,0,1:T(8,128)(2,1)S(1)} %copy.77), channel_id=1, replica_groups=mesh['ep'=16,'tp'=32] {'ep'}, dimensions={1} | all-to-all | bytes 524288 | tf_op jit(solution)/shard_map/all_to_all | solution.py:46
  26.4 0.7 copy.78
  27.1 0.0 all-gather.3.cloned.1.call-update
  27.1 0.0 all-gather.5.cloned.1.call-start
  27.2 98.1 %all-gather.3.cloned.1.call-done = bf16[2,512,4096]{2,1,0:T(8,128)(2,1)} async-done(((bf16[2,512,128]{2,1,0:T(8,128)(2,1)}), bf16[2,512,4096]{2,1,0:T(8,128)(2,1)}) %all-gather.3.cloned.1.call-update) | async-done | bytes 8388624 | tf_op jit(solution)/shard_map/all_gather | solution.py:49
  125.2 5.2 %fusion = f32[2,512]{1,0:T(2,128)S(1)} fusion(bf16[2,512,4096]{2,1,0:T(8,128)(2,1)} %all-gather.3.cloned.1.call-done), kind=kLoop, calls=%fused_computation.2 | loop fusion | flops 12581888 | bytes 8392704 | tf_op jit(solution)/shard_map/esn,esn->es/dot_general | solution.py:52
  130.5 0.5 copy-done.1
  131.0 2.6 %fusion.3 = f32[2,32,512]{2,1,0:T(8,128)S(1)} fusion(bf16[2,512,4096]{2,1,0:T(8,128)(2,1)S(1)} %copy-done.1, bf16[2,32,4096]{2,1,0:T(8,128)(2,1)S(1)} %copy-done.2, f32[2,512]{1,0:T(2,128)S(1)} %add_rsqrt_fusion), kind=kOutput, calls=%fused_computation.10 | convolution fusion | flops 268468224 | bytes 9048064 | tf_op jit(solution)/shard_map/efn,esn->efs/dot_general | solution.py:50
  133.7 3.2 %fusion.5 = bf16[2,32,512]{2,1,0:T(8,128)(2,1)} fusion(bf16[2,512,4096]{2,1,0:T(8,128)(2,1)S(1)} %copy-done.1, bf16[2,32,4096]{2,1,0:T(8,128)(2,1)S(1)} %copy-done.3, f32[2,32,512]{2,1,0:T(8,128)S(1)} %fusion.3, f32[2,512]{1,0:T(2,128)S(1)} %add_rsqrt_fusion), kind=kOutput, calls=%fused_computation.12 | convolution fusion | flops 268664832 | bytes 9113600 | tf_op jit(solution)/shard_map/efn,esn->efs/dot_general | solution.py:51
  136.9 0.1 reshape.209
  137.0 0.1 copy.82
  137.2 67.7 %all-gather.5.cloned.1.call-done = bf16[2,1024,512]{2,1,0:T(8,128)(2,1)} async-done(((bf16[2,32,512]{2,1,0:T(8,128)(2,1)}), bf16[2,1024,512]{2,1,0:T(8,128)(2,1)}) %all-gather.5.cloned.1.call-update) | async-done | bytes 2097168 | tf_op jit(solution)/shard_map/all_gather | solution.py:60
  204.9 2.5 convolution_convert_fusion
  207.4 0.7 copy.79
  208.1 6.5 %all-to-all-start.1 = ((bf16[2,16,32,128]{3,2,0,1:T(8,128)(2,1)}), bf16[2,16,32,128]{3,2,0,1:T(8,128)(2,1)S(1)}, u32[]{:S(2)}, u32[]{:S(2)}) async-start(bf16[2,16,32,128]{3,2,0,1:T(8,128)(2,1)} %copy.79), calls=%async_computation.1 | async-start | bytes 524288 | tf_op jit(solution)/shard_map/all_to_all | solution.py:64
  214.7 8.2 %all-to-all-done.1 = bf16[2,16,32,128]{3,2,0,1:T(8,128)(2,1)S(1)} async-done(((bf16[2,16,32,128]{3,2,0,1:T(8,128)(2,1)}), bf16[2,16,32,128]{3,2,0,1:T(8,128)(2,1)S(1)}, u32[]{:S(2)}, u32[]{:S(2)}) %all-to-all-start.1) | async-done | bytes 262176 | tf_op jit(solution)/shard_map/all_to_all | solution.py:64
  222.9 1.3 gather_fusion
  224.2 0.2 fusion.6
  224.5 0.1 multiply_reduce_fusion
  224.6 21.2 %all_to_all.17 = f32[32,1,128]{2,1,0:T(1,128)S(1)} all-to-all(f32[32,1,128]{2,1,0:T(1,128)S(1)} %broadcast_in_dim.2), channel_id=1, replica_groups=mesh['ep'=16,'tp'=32] {'tp'}, dimensions={0} | all-to-all | bytes 32768 | tf_op jit(solution)/shard_map/all_to_all | solution.py:14
  245.9 0.7 multiply_convert_fusion
  (24 shorter events, 0.2 us)
Async XLA Ops:
  6.5 198.4 %copy-start = (bf16[2,1024,128]{2,1,0:T(8,128)(2,1)S(1)}, bf16[2,1024,128]{2,1,0:T(8,128)(2,1)}, u32[]{:S(2)}) copy-start(bf16[2,1024,128]{2,1,0:T(8,128)(2,1)} %param.12) | copy-start | bytes 1572868
  6.5 124.0 %copy-start.2 = (bf16[2,32,4096]{2,1,0:T(8,128)(2,1)S(1)}, bf16[2,32,4096]{2,1,0:T(8,128)(2,1)}, u32[]{:S(2)}) copy-start(bf16[2,32,4096]{2,1,0:T(8,128)(2,1)} %param.10) | copy-start | bytes 1572868
  6.5 118.7 %all-gather.3.cloned.1.call-start = ((), (), s32[]{:S(2)}) async-start(), calls=%async_computation.3 | async-start | bytes 8650752 | tf_op jit(solution)/shard_map/all_gather | solution.py:49
  27.1 177.8 %all-gather.5.cloned.1.call-start = ((), (), s32[]{:S(2)}) async-start(), calls=%async_computation.4 | async-start | bytes 2162688 | tf_op jit(solution)/shard_map/all_gather | solution.py:60
  125.2 5.8 %copy-start.1 = (bf16[2,512,4096]{2,1,0:T(8,128)(2,1)S(1)}, bf16[2,512,4096]{2,1,0:T(8,128)(2,1)}, u32[]{:S(2)}) copy-start(bf16[2,512,4096]{2,1,0:T(8,128)(2,1)} %all-gather.3.cloned.1.call-done) | copy-start | bytes 25165828
  125.2 8.4 %copy-start.3 = (bf16[2,32,4096]{2,1,0:T(8,128)(2,1)S(1)}, bf16[2,32,4096]{2,1,0:T(8,128)(2,1)}, u32[]{:S(2)}) copy-start(bf16[2,32,4096]{2,1,0:T(8,128)(2,1)} %param.11) | copy-start | bytes 1572868
  131.0 6.0 %copy-start.4 = (f32[128,4]{0,1:T(4,128)S(1)}, f32[128,4]{0,1:T(4,128)}, u32[]{:S(2)}) copy-start(f32[128,4]{0,1:T(4,128)} %param.9) | copy-start | bytes 6148
  133.7 112.2 %copy-start.5 = (f32[128]{0:T(128)S(1)}, f32[128]{0:T(128)}, u32[]{:S(2)}) copy-start(f32[128]{0:T(128)} %param.13) | copy-start | bytes 1540
  208.1 14.7 %all-to-all-start.1 = ((bf16[2,16,32,128]{3,2,0,1:T(8,128)(2,1)}), bf16[2,16,32,128]{3,2,0,1:T(8,128)(2,1)S(1)}, u32[]{:S(2)}, u32[]{:S(2)}) async-start(bf16[2,16,32,128]{3,2,0,1:T(8,128)(2,1)} %copy.79), calls=%async_computation.1 | async-start | bytes 524288 | tf_op jit(solution)/shard_map/all_to_all | solution.py:64
Sparse Core Ops, SparseCore 0:
  27.2 97.9 all-gather.2
  137.0 67.7 all-gather.4
where the time goes:
time: 254 us; the launch traced here: 253 us
  waiting for transfers between devices  174 us (69%)
  blocking collectives  36.1 us (14%)
  between operations  13.5 us (5%)
  matrix products  9.35 us (4%)
  other arithmetic  8.73 us (3%)
  starting transfers between devices  6.57 us (3%)
  local copies, waits for them, and re-layouts  5.09 us (2%)
    all_gather x1, waiting for transfers between devices, body(): piece_cols = lax.all_gather(arrived, 'tp', axis=2, tiled=True)  98.1 us
    all_gather x1, waiting for transfers between devices, body(): lax.all_gather(hidden, 'tp', axis=1, tiled=True)  67.7 us
    all_to_all x1, blocking collectives, from_everyone(): lax.all_to_all(jnp.broadcast_to(value[None], (length, *value.shape)), axi...  21.2 us
    all_to_all x1, blocking collectives, body(): lax.all_to_all(outgoing, 'ep', split_axis=1, concat_axis=1, tiled=True)  14.9 us
    all_to_all x1, waiting for transfers between devices, body(): lax.all_to_all(expert_out.reshape(EXP_DEV, ep_count, slot_count, out_part...  8.16 us
    all_to_all x1, starting transfers between devices, body(): lax.all_to_all(expert_out.reshape(EXP_DEV, ep_count, slot_count, out_part...  6.53 us
    dot_general x1, other arithmetic, body(): jnp.einsum('esn,esn->es', piece_cols, piece_cols, preferred_element_type=...  5.23 us
  transfers between devices with their start and end apart: 3, of which 3 were waited for; matrix products, arithmetic and copies ran while one was open for 0% of the time, Pallas kernels for 0%

commit v1 on v0

--- a/solution.py
+++ b/solution.py
@@ -46,7 +46,7 @@
     arrived = lax.all_to_all(outgoing, "ep", split_axis=1, concat_axis=1, tiled=True).reshape(
         EXP_DEV, span_rows, width_part
     )
-    piece_cols = lax.all_gather(arrived, "tp", axis=2, tiled=True)
+    piece_cols = jnp.concatenate(lax.all_gather(arrived, "tp"), axis=2)
     gate_sum = jnp.einsum("efn,esn->efs", w_gate, piece_cols, preferred_element_type=jnp.float32)
     up_sum = jnp.einsum("efn,esn->efs", w_up, piece_cols, preferred_element_type=jnp.float32)
     square_sum = jnp.einsum(

time: 254 us -> 237 us (0.933)
  waiting for transfers between devices: 174 us -> 158 us
    all_gather x1, waiting for transfers between devices: 98.1 us -> 81.2 us  [body(): piece_cols = jnp.concatenate(lax.all_gather(arrived, 'tp'), axis=2)]
where the time goes in v1:
time: 237 us
  waiting for transfers between devices  158 us (67%)
  blocking collectives  36.1 us (15%)
  between operations  13.5 us (6%)
  matrix products  9.17 us (4%)
  other arithmetic  8.73 us (4%)
  starting transfers between devices  6.57 us (3%)
  local copies, waits for them, and re-layouts  5.09 us (2%)
    all_gather x1, waiting for transfers between devices, body(): piece_cols = jnp.concatenate(lax.all_gather(arrived, 'tp'), axis=2)  81.2 us
    all_gather x1, waiting for transfers between devices, body(): lax.all_gather(hidden, 'tp', axis=1, tiled=True)  68.1 us
    all_to_all x1, blocking collectives, from_everyone(): lax.all_to_all(jnp.broadcast_to(value[None], (length, *value.shape)), axi...  21.2 us
    all_to_all x1, blocking collectives, body(): lax.all_to_all(outgoing, 'ep', split_axis=1, concat_axis=1, tiled=True)  14.9 us
    all_to_all x1, waiting for transfers between devices, body(): lax.all_to_all(expert_out.reshape(EXP_DEV, ep_count, slot_count, out_part...  8.16 us
    all_to_all x1, starting transfers between devices, body(): lax.all_to_all(expert_out.reshape(EXP_DEV, ep_count, slot_count, out_part...  6.53 us
    dot_general x1, other arithmetic, body(): jnp.einsum('esn,esn->es', piece_cols, piece_cols, preferred_element_type=...  5.23 us
  transfers between devices with their start and end apart: 3, of which 3 were waited for; matrix products, arithmetic and copies ran while one was open for 0% of the time, Pallas kernels for 0%

profile of v1, /device:TPU:1, one launch (start us, length us, event | category | flops | bytes accessed | tf_op | source)
XLA Modules:
  0.0 236.8 jit_solution(8803433938441525516)
XLA Ops:
  6.5 0.9 copy.94
  7.4 0.1 eq.44
  7.5 0.1 eq.40
  7.6 1.2 reduce-window.6
  8.8 0.2 slice_reduce_fusion
  9.1 0.1 fusion.29
  9.2 0.1 reduce_sum.41
  9.3 0.1 copy.97
  9.4 0.7 fusion.33
  10.1 0.4 fusion.7
  10.4 1.0 convolution_convert_fusion.1
  11.5 14.9 %all_to_all.16 = bf16[2,16,32,128]{3,2,0,1:T(8,128)(2,1)S(1)} all-to-all(bf16[2,16,32,128]{3,2,0,1:T(8,128)(2,1)S(1)} %copy.98), channel_id=1, replica_groups=mesh['ep'=16,'tp'=32] {'ep'}, dimensions={1} | all-to-all | bytes 524288 | tf_op jit(solution)/shard_map/all_to_all | solution.py:46
  26.4 0.7 copy.99
  27.1 0.0 all-gather.5.cloned.1.call-start
  27.2 81.2 %all-gather.3.cloned.1.call-done = bf16[32,2,512,128]{3,2,1,0:T(8,128)(2,1)} async-done(((bf16[1,2,512,128]{3,2,1,0:T(8,128)(2,1)}), bf16[32,2,512,128]{3,2,1,0:T(8,128)(2,1)}) %all-gather.3.cloned.1.call-update) | async-done | bytes 8388624 | tf_op jit(solution)/shard_map/all_gather | solution.py:49
  108.4 5.2 %fusion = f32[2,512]{1,0:T(2,128)S(1)} fusion(bf16[32,2,512,128]{3,2,1,0:T(8,128)(2,1)} %all-gather.3.cloned.1.call-done), kind=kLoop, calls=%fused_computation.2 | loop fusion | flops 12581888 | bytes 8392704 | tf_op jit(solution)/shard_map/esn,esn->es/dot_general | solution.py:52
  113.7 0.5 copy-done.1
  114.2 2.5 %fusion.11 = f32[2,32,512]{2,1,0:T(8,128)S(1)} fusion(bf16[2,32,4096]{2,1,0:T(8,128)(2,1)S(1)} %copy-done.4, f32[2,512]{1,0:T(2,128)S(1)} %add_rsqrt_fusion, bf16[32,2,512,128]{3,2,1,0:T(8,128)(2,1)S(1)} %copy-done.1), kind=kOutput, calls=%fused_computation.14 | convolution fusion | flops 268468224 | bytes 9048064 | tf_op jit(solution)/shard_map/efn,esn->efs/dot_general | solution.py:50
  116.7 0.0 copy-done.5
  116.7 3.2 %fusion.23 = bf16[2,32,512]{2,1,0:T(8,128)(2,1)} fusion(bf16[2,32,4096]{2,1,0:T(8,128)(2,1)S(1)} %copy-done.5, f32[2,32,512]{2,1,0:T(8,128)S(1)} %fusion.11, f32[2,512]{1,0:T(2,128)S(1)} %add_rsqrt_fusion, bf16[32,2,512,128]{3,2,1,0:T(8,128)(2,1)S(1)} %copy-done.1), kind=kOutput, calls=%fused_computation.18 | convolution fusion | flops 268664832 | bytes 9113600 | tf_op jit(solution)/shard_map/efn,esn->efs/dot_general | solution.py:51
  119.9 0.1 reshape.213
  120.0 0.1 copy.104
  120.2 68.1 %all-gather.5.cloned.1.call-done = bf16[2,1024,512]{2,1,0:T(8,128)(2,1)} async-done(((bf16[2,32,512]{2,1,0:T(8,128)(2,1)}), bf16[2,1024,512]{2,1,0:T(8,128)(2,1)}) %all-gather.5.cloned.1.call-update) | async-done | bytes 2097168 | tf_op jit(solution)/shard_map/all_gather | solution.py:60
  188.2 2.5 %convolution_convert_fusion = bf16[2,512,128]{2,1,0:T(8,128)(2,1)S(1)} fusion(bf16[2,1024,512]{2,1,0:T(8,128)(2,1)} %all-gather.5.cloned.1.call-done, bf16[2,1024,128]{2,1,0:T(8,128)(2,1)S(1)} %copy-done), kind=kOutput, calls=%fused_computation.11 | convolution fusion | flops 268566528 | bytes 2883584 | tf_op jit(solution)/shard_map/ens,end->esd/dot_general | solution.py:58
  190.8 0.7 copy.101
  191.5 6.5 %all-to-all-start.1 = ((bf16[2,16,32,128]{3,2,0,1:T(8,128)(2,1)}), bf16[2,16,32,128]{3,2,0,1:T(8,128)(2,1)S(1)}, u32[]{:S(2)}, u32[]{:S(2)}) async-start(bf16[2,16,32,128]{3,2,0,1:T(8,128)(2,1)} %copy.101), calls=%async_computation.1 | async-start | bytes 524288 | tf_op jit(solution)/shard_map/all_to_all | solution.py:64
  198.1 8.2 %all-to-all-done.1 = bf16[2,16,32,128]{3,2,0,1:T(8,128)(2,1)S(1)} async-done(((bf16[2,16,32,128]{3,2,0,1:T(8,128)(2,1)}), bf16[2,16,32,128]{3,2,0,1:T(8,128)(2,1)S(1)}, u32[]{:S(2)}, u32[]{:S(2)}) %all-to-all-start.1) | async-done | bytes 262176 | tf_op jit(solution)/shard_map/all_to_all | solution.py:64
  206.2 1.3 gather_fusion
  207.6 0.2 fusion.26
  207.8 0.1 multiply_reduce_fusion
  208.0 21.2 %all_to_all.17 = f32[32,1,128]{2,1,0:T(1,128)S(1)} all-to-all(f32[32,1,128]{2,1,0:T(1,128)S(1)} %broadcast_in_dim.2), channel_id=1, replica_groups=mesh['ep'=16,'tp'=32] {'tp'}, dimensions={0} | all-to-all | bytes 32768 | tf_op jit(solution)/shard_map/all_to_all | solution.py:14
  229.2 0.7 multiply_convert_fusion
  (24 shorter events, 0.2 us)
Async XLA Ops:
  6.5 181.7 %copy-start = (bf16[2,1024,128]{2,1,0:T(8,128)(2,1)S(1)}, bf16[2,1024,128]{2,1,0:T(8,128)(2,1)}, u32[]{:S(2)}) copy-start(bf16[2,1024,128]{2,1,0:T(8,128)(2,1)} %param.12) | copy-start | bytes 1572868
  6.5 107.1 %copy-start.4 = (bf16[2,32,4096]{2,1,0:T(8,128)(2,1)S(1)}, bf16[2,32,4096]{2,1,0:T(8,128)(2,1)}, u32[]{:S(2)}) copy-start(bf16[2,32,4096]{2,1,0:T(8,128)(2,1)} %param.10) | copy-start | bytes 1572868
  6.5 101.9 %all-gather.3.cloned.1.call-start = ((), (), s32[]{:S(2)}) async-start(), calls=%async_computation.3 | async-start | bytes 8650752 | tf_op jit(solution)/shard_map/all_gather | solution.py:49
  27.1 161.1 %all-gather.5.cloned.1.call-start = ((), (), s32[]{:S(2)}) async-start(), calls=%async_computation.4 | async-start | bytes 2162688 | tf_op jit(solution)/shard_map/all_gather | solution.py:60
  108.4 5.8 %copy-start.1 = (bf16[32,2,512,128]{3,2,1,0:T(8,128)(2,1)S(1)}, bf16[32,2,512,128]{3,2,1,0:T(8,128)(2,1)}, u32[]{:S(2)}) copy-start(bf16[32,2,512,128]{3,2,1,0:T(8,128)(2,1)} %all-gather.3.cloned.1.call-done) | copy-start | bytes 25165828
  108.4 8.3 %copy-start.5 = (bf16[2,32,4096]{2,1,0:T(8,128)(2,1)S(1)}, bf16[2,32,4096]{2,1,0:T(8,128)(2,1)}, u32[]{:S(2)}) copy-start(bf16[2,32,4096]{2,1,0:T(8,128)(2,1)} %param.11) | copy-start | bytes 1572868
  116.7 3.3 %copy-start.2 = (f32[128,4]{0,1:T(4,128)S(1)}, f32[128,4]{0,1:T(4,128)}, u32[]{:S(2)}) copy-start(f32[128,4]{0,1:T(4,128)} %param.9) | copy-start | bytes 6148
  116.7 112.5 %copy-start.3 = (f32[128]{0:T(128)S(1)}, f32[128]{0:T(128)}, u32[]{:S(2)}) copy-start(f32[128]{0:T(128)} %param.13) | copy-start | bytes 1540
  191.5 14.7 %all-to-all-start.1 = ((bf16[2,16,32,128]{3,2,0,1:T(8,128)(2,1)}), bf16[2,16,32,128]{3,2,0,1:T(8,128)(2,1)S(1)}, u32[]{:S(2)}, u32[]{:S(2)}) async-start(bf16[2,16,32,128]{3,2,0,1:T(8,128)(2,1)} %copy.101), calls=%async_computation.1 | async-start | bytes 524288 | tf_op jit(solution)/shard_map/all_to_all | solution.py:64
Sparse Core Ops, SparseCore 0:
  27.2 81.1 all-gather.2
  120.0 68.1 all-gather.4
